TPU v7x, 32 devices: a whole 2x2x4 slice. The times are simulated.
32 devices in a mesh: grp: 2 (over y), kv: 4 (over z), tp: 4 (over x, core).
Axes of the slice: x: 2, y: 2, z: 4, core: 2. Of those that a mesh axis runs over, the one named last changes fastest.
Arguments:
- tokens: bfloat16 [256, 4096], P('grp', 'kv'), parts along dimension 0, may hold values from -36 to 36
- span_lengths: int32 [256], P(('grp', 'kv')), parts along dimension 0, may hold values from 1 to 256, 13107 in all
- block_state: float32 [256, 64, 32, 64], P(('grp', 'kv'), 'tp'), parts along dimension 0, may hold values from -96 to 96
- key_cache: bfloat16 [256, 2048, 256], P(('grp', 'kv'), 'tp'), parts along dimension 0, may hold values from -6 to 6
- value_cache: bfloat16 [256, 4096, 256], P(('grp', 'kv'), 'tp'), parts along dimension 0, may hold values from -6 to 6
- decay_cache: float32 [256, 2048, 256], P(('grp', 'kv'), 'tp'), parts along dimension 0, may hold values from -34 to 0, as said below
- attn_gain: float32 [4096], P('kv'), may hold values from 0.1 to 1.9
- query_weight: bfloat16 [4096, 2048], P('kv', 'tp'), may hold values from -0.09375 to 0.09375
- key_weight: bfloat16 [4096, 2048], P('kv', 'tp'), may hold values from -0.09375 to 0.09375
- value_weight: bfloat16 [4096, 4096], P('kv', 'tp'), may hold values from -0.09375 to 0.09375
- gate_weight: bfloat16 [4096, 4096], P('kv', 'tp'), may hold values from -0.09375 to 0.09375
- decay_matrix: bfloat16 [4096, 2048], P('kv', 'tp'), may hold values from -0.09375 to 0.09375
- decay_offset_bias: float32 [2048], P('tp'), may hold values from -1.4 to 6
- head_gain: float32 [64], replicated, may hold values from 0.1 to 1.9
- out_weight: bfloat16 [4096, 4096], P('tp', 'kv'), may hold values from -0.09375 to 0.09375
- mixer_gain: float32 [4096], P('kv'), may hold values from 0.1 to 1.9
- up_weight: bfloat16 [4096, 16384], P('kv', 'tp'), may hold values from -0.09375 to 0.09375
- down_weight: bfloat16 [16384, 4096], P('tp', 'kv'), may hold values from -0.046875 to 0.046875
Outputs:
- layer_out: bfloat16 [256, 4096], P('grp', 'kv'), parts along dimension 0
There are 2 independent parts, one for each index of `grp`. A program takes and returns all parts, laid end to end along the dimension named above; an argument that names none is the same for every part. Nothing has to cross between parts.
Inputs may be any that keep to these rules, and one draw needn't show every extreme that they name: Cached positions at index span_lengths - 1 and beyond are unused. `decay_cache`: Non-increasing along positions.
All inputs are finite; a program needn't handle non-finite values. No bound on the sum of `span_lengths` on one device may be relied on, other than what follows from the above.
Results may differ from a plain program's by a relative error of at most 0.005.
The roundings to bfloat16 on the way count: a program that leaves them out, or rounds other values in their place, can miss the bound.
Values may be sent and summed in bfloat16 or wider, within the bound.
A program may use at most 128 MiB of HBM per device.

v0:
```python
import jax
import jax.numpy as jnp
from jax import lax
from jax.sharding import PartitionSpec as P

D = 4096
KEY_WIDTH = 32
DV = 64
NORM_EPS = 1e-06
DECAY_SOFTNESS = 16.0


def shards(
    tokens,
    span_lengths,
    block_state,
    key_cache,
    value_cache,
    decay_cache,
    attn_gain,
    query_weight,
    key_weight,
    value_weight,
    gate_weight,
    decay_matrix,
    decay_offset_bias,
    head_gain,
    out_weight,
    mixer_gain,
    up_weight,
    down_weight,
):
    seq_count = block_state.shape[0]
    head_count = block_state.shape[1]
    span_size = key_cache.shape[2]
    whole_rows = tokens.astype(jnp.float32)
    square_sum = jnp.sum(whole_rows * whole_rows, axis=1)
    scaled = (whole_rows * attn_gain).astype(jnp.bfloat16)
    query_part = jnp.dot(scaled, query_weight, preferred_element_type=jnp.float32)
    key_part = jnp.dot(scaled, key_weight, preferred_element_type=jnp.float32)
    value_part = jnp.dot(scaled, value_weight, preferred_element_type=jnp.float32)
    gate_part = jnp.dot(scaled, gate_weight, preferred_element_type=jnp.float32)
    decay_part = jnp.dot(scaled, decay_matrix, preferred_element_type=jnp.float32)
    square_total = lax.psum(square_sum, "kv")
    query_sum, key_sum, value_sum, gate_sum, decay_running_sum = (
        lax.psum_scatter(query_part, "kv", scatter_dimension=0, tiled=True),
        lax.psum_scatter(key_part, "kv", scatter_dimension=0, tiled=True),
        lax.psum_scatter(value_part, "kv", scatter_dimension=0, tiled=True),
        lax.psum_scatter(gate_part, "kv", scatter_dimension=0, tiled=True),
        lax.psum_scatter(decay_part, "kv", scatter_dimension=0, tiled=True),
    )
    own_square = lax.dynamic_slice_in_dim(square_total, lax.axis_index("kv") * seq_count, seq_count)
    scale_per_row = lax.rsqrt(own_square / D + NORM_EPS)[:, None]
    query = (query_sum * scale_per_row * KEY_WIDTH ** (-0.5)).reshape(
        seq_count, head_count, KEY_WIDTH
    )
    key_new = (key_sum * scale_per_row).reshape(seq_count, head_count, KEY_WIDTH)
    value_new = (value_sum * scale_per_row).reshape(seq_count, head_count, DV)
    gate = gate_sum * scale_per_row
    logarithm_decay = (
        jax.nn.log_sigmoid(decay_running_sum * scale_per_row + decay_offset_bias) / DECAY_SOFTNESS
    )
    token_place = lax.broadcasted_iota(jnp.int32, (1, 1, span_size), 2)
    lengths_now = span_lengths[:, None, None]
    previous = jnp.sum(jnp.where(token_place == lengths_now - 2, decay_cache, 0.0), axis=-1)
    now_decay = (previous + logarithm_decay).reshape(seq_count, head_count, KEY_WIDTH)
    decays_span = decay_cache.reshape(seq_count, head_count, KEY_WIDTH, span_size)
    in_use = (token_place < lengths_now - 1)[:, :, None, :]
    factor = jnp.where(in_use, jnp.exp(now_decay[..., None] - decays_span), 0.0)
    keys_span = key_cache.reshape(seq_count, head_count, KEY_WIDTH, span_size)
    scores = jnp.sum(query[..., None] * keys_span.astype(jnp.float32) * factor, axis=2)
    scores_low = scores.astype(jnp.bfloat16)
    values_span = value_cache.reshape(seq_count, head_count, DV, span_size)
    history = jnp.einsum(
        "nhs,nhvs->nhv", scores_low, values_span, preferred_element_type=jnp.float32
    )
    carried = jnp.einsum(
        "nhc,nhcv->nhv", query * jnp.exp(now_decay), block_state, precision=lax.Precision.HIGHEST
    )
    own_term = jnp.sum(query * key_new, axis=-1, keepdims=True) * value_new
    raw = carried + history + own_term
    normed = raw * lax.rsqrt(jnp.mean(raw * raw, axis=-1, keepdims=True) + NORM_EPS) * head_gain
    mixed = (normed.reshape(seq_count, head_count * DV) * jax.nn.silu(gate)).astype(jnp.bfloat16)
    attn_terms = jnp.dot(
        lax.all_gather(mixed, "kv", axis=0, tiled=True),
        out_weight,
        preferred_element_type=jnp.float32,
    )
    attn_out = lax.psum(attn_terms, "tp")
    resid = (whole_rows + attn_out).astype(jnp.bfloat16)
    resid_rows = resid.astype(jnp.float32)
    mixer_square = jnp.sum(resid_rows * resid_rows, axis=1)
    mixer_scaled = (resid_rows * mixer_gain).astype(jnp.bfloat16)
    up_part = jnp.dot(mixer_scaled, up_weight, preferred_element_type=jnp.float32)
    up_share, square_share = (
        lax.psum_scatter(up_part, "kv", scatter_dimension=0, tiled=True),
        lax.psum_scatter(mixer_square, "kv", scatter_dimension=0, tiled=True),
    )
    hidden_share = jnp.square(
        jax.nn.relu(up_share * lax.rsqrt(square_share / D + NORM_EPS)[:, None])
    )
    hidden_share = hidden_share.astype(jnp.bfloat16)
    down_terms = jnp.dot(
        lax.all_gather(hidden_share, "kv", axis=0, tiled=True),
        down_weight,
        preferred_element_type=jnp.float32,
    )
    mixer_out = lax.psum(down_terms, "tp")
    return (resid_rows + mixer_out).astype(jnp.bfloat16)


def solution(mesh):
    placed = (
        P("grp", "kv"),
        P(("grp", "kv")),
        P(("grp", "kv"), "tp", None, None),
        P(("grp", "kv"), "tp", None),
        P(("grp", "kv"), "tp", None),
        P(("grp", "kv"), "tp", None),
        P("kv"),
        P("kv", "tp"),
        P("kv", "tp"),
        P("kv", "tp"),
        P("kv", "tp"),
        P("kv", "tp"),
        P("tp"),
        P(),
        P("tp", "kv"),
        P("kv"),
        P("kv", "tp"),
        P("tp", "kv"),
    )
    return jax.shard_map(
        shards, mesh=mesh, in_specs=placed, out_specs=P("grp", "kv"), check_vma=False
    )
```

profile of v0, /device:TPU:0, one launch (start us, length us, event | category | flops | bytes accessed | tf_op | source)
XLA Modules:
  0.0 293.3 jit_solution(13781271329002494492)
XLA Ops:
  6.5 0.0 reduce-scatter.7.cloned.1.call-start
  6.6 2.5 fusion.21
  9.1 0.0 reduce-scatter.7.cloned.1.call-update
  9.1 0.0 reduce-scatter.11.cloned.1.call-start
  9.2 2.4 fusion.17
  11.5 0.0 reduce-scatter.11.cloned.1.call-update
  11.5 0.0 reduce-scatter.9.cloned.1.call-start
  11.6 2.3 fusion.19
  13.9 0.0 reduce-scatter.9.cloned.1.call-update
  14.0 0.0 reduce-scatter.13.cloned.1.call-start
  14.0 2.2 fusion.15
  16.2 0.0 reduce-scatter.13.cloned.1.call-update
  16.2 0.0 reduce-scatter.15.cloned.1.call-start
  16.3 2.9 fusion.13
  19.2 0.0 reduce-scatter.15.cloned.1.call-update
  19.2 0.0 all-reduce.4.cloned.1.call-start
  19.2 0.1 fusion.3
  19.4 13.6 %psum.21 = f32[128]{0:T(128)S(1)} all-reduce(f32[128]{0:T(128)S(1)} %fusion.3), channel_id=1, replica_groups=mesh['grp'=2,'kv'=4,'tp'=4] {'kv'}, use_global_device_ids=true, to_apply=%region_2.0 | all-reduce | flops 128 | bytes 1024 | tf_op jit(solution)/shard_map/psum | solution.py:44
  33.0 0.1 iota_compare_fusion
  33.0 0.1 iota_compare_fusion.1
  33.1 0.1 add_rsqrt_fusion.1
  33.2 8.0 %select_reduce_fusion = f32[32,512]{1,0:T(8,128)S(1)} fusion(f32[32,512,256]{2,1,0:T(8,128)} %param.23, pred[32,256]{1,0:T(8,128)(4,1)S(1)} %iota_compare_fusion.1), kind=kLoop, calls=%fused_computation.3 | loop fusion | flops 8372224 | bytes 16850944 | tf_op jit(solution)/shard_map/reduce_sum | solution.py:65
  41.2 0.0 reduce-scatter.7.cloned.1.call-done
  41.3 11.6 %reduce-scatter.11.cloned.1.call-done = f32[32,512]{1,0:T(8,128)} async-done(((f32[128,512]{1,0:T(8,128)}), f32[32,512]{1,0:T(8,128)}) %reduce-scatter.11.cloned.1.call-update) | async-done | bytes 65552 | tf_op jit(solution)/shard_map/reduce_scatter | solution.py:47
  52.9 20.5 %reduce-scatter.9.cloned.1.call-done = f32[32,512]{1,0:T(8,128)} async-done(((f32[128,512]{1,0:T(8,128)}), f32[32,512]{1,0:T(8,128)}) %reduce-scatter.9.cloned.1.call-update) | async-done | bytes 65552 | tf_op jit(solution)/shard_map/reduce_scatter | solution.py:50
  73.5 1.0 fusion.25
  74.5 0.1 reshape.83
  74.6 0.1 reshape.82
  74.7 0.1 reshape.86
  74.8 0.1 exponential_multiply_fusion
  75.0 9.7 %fusion.1 = bf16[32,16,256]{2,1,0:T(8,128)(2,1)S(1)} fusion(f32[32,16,32]{2,1,0:T(8,128)S(1)} %reshape.83, f32[32,16,32]{2,1,0:T(8,128)S(1)} %reshape.82, pred[32,256]{1,0:T(8,128)(4,1)S(1)} %iota_compare_fusion, bf16[32,512,256]{2,1,0:T(8,128)(2,1)} %param.21, f32[32,512,256]{2,1,0:T(8,128)} %param.23), kind=kLoop, calls=%fused_computation.2 | loop fusion | flops 25034752 | bytes 25567232 | tf_op jit(solution)/shard_map/reduce_sum | solution.py:71
  84.7 10.3 %fusion.8 = f32[32,16,1,64]{3,2,1,0:T(1,128)S(1)} fusion(bf16[32,16,64,256]{3,2,1,0:T(8,128)(2,1)} %bitcast.34, bf16[32,16,256,1]{2,1,0,3:T(8,128)(2,1)S(1)} %bitcast.32), kind=kOutput, calls=%fused_computation.16 | convolution fusion | flops 16777216 | bytes 17170432 | tf_op jit(solution)/shard_map/nhs,nhvs->nhv/dot_general | solution.py:74
  94.9 9.2 %fusion.29 = f32[32,16,1,64]{3,2,1,0:T(1,128)S(1)} fusion(f32[32,16,32,1]{2,3,1,0:T(1,128)S(1)} %bitcast.31, f32[32,16,32,64]{3,2,1,0:T(8,128)} %param.20), kind=kOutput, calls=%fused_computation.49 | convolution fusion | flops 12582912 | bytes 4390912 | tf_op jit(solution)/shard_map/nhc,nhcv->nhv/dot_general | solution.py:77
  104.2 0.0 reduce-scatter.13.cloned.1.call-done
  104.2 1.0 broadcast_multiply_fusion
  105.2 0.1 reshape.87
  105.3 0.2 multiply_reduce_fusion
  105.6 0.1 multiply_multiply_fusion
  105.7 0.1 reshape.88
  105.8 12.1 %reduce-scatter.15.cloned.1.call-done = f32[32,1024]{1,0:T(8,128)} async-done(((f32[128,1024]{1,0:T(8,128)}), f32[32,1024]{1,0:T(8,128)}) %reduce-scatter.15.cloned.1.call-update) | async-done | bytes 131088 | tf_op jit(solution)/shard_map/reduce_scatter | solution.py:49
  118.0 1.0 multiply_convert_fusion.1
  119.0 13.8 %all_gather.6 = bf16[128,1024]{1,0:T(8,128)(2,1)S(1)} all-gather(bf16[32,1024]{1,0:T(8,128)(2,1)S(1)} %multiply_convert_fusion.1), channel_id=1, replica_groups=mesh['grp'=2,'kv'=4,'tp'=4] {'kv'}, dimensions={0}, use_global_device_ids=true | all-gather | bytes 327680 | tf_op jit(solution)/shard_map/all_gather | solution.py:85
  132.8 1.3 fusion.30
  134.0 0.0 all-reduce.4.cloned.1.call-update
  134.1 0.2 reduce-scatter.17.cloned.1.call-start
  134.3 31.5 %all-reduce.4.cloned.1.call-done = f32[128,1024]{1,0:T(8,128)} async-done(((f32[128,1024]{1,0:T(8,128)}), f32[128,1024]{1,0:T(8,128)}) %all-reduce.4.cloned.1.call-update) | async-done | bytes 524304 | tf_op jit(solution)/shard_map/psum | solution.py:89
  165.8 1.2 fusion.6
  167.0 0.0 copy-start.9
  167.0 6.0 %fusion.10 = f32[128,4096]{1,0:T(8,128)} fusion(bf16[1024,4096]{1,0:T(8,128)(2,1)} %param.34, bf16[128,1024]{1,0:T(8,128)(2,1)S(1)} %get-tuple-element.6, f32[1024]{0:T(1024)S(1)} %copy-done.5), kind=kOutput, calls=%fused_computation.19 | convolution fusion | flops 1074135040 | bytes 10752000 | tf_op jit(solution)/shard_map/dot_general | solution.py:94
  173.0 0.0 reduce-scatter.17.cloned.1.call-update
  173.1 0.0 all-gather.2.cloned.1.call-start
  173.1 0.6 dynamic-slice
  174.4 12.1 %all-reduce = f32[128]{0:T(128)S(1)} all-reduce(f32[128]{0:T(128)S(1)} %get-tuple-element.5), channel_id=8, replica_groups=mesh['grp'=2,'kv'=4,'tp'=4] {'kv'}, use_global_device_ids=true, to_apply=%region_14.15.clone | all-reduce | flops 128 | bytes 1024
  186.4 0.1 fusion.27
  186.5 30.4 %reduce-scatter.17.cloned.1.call-done = f32[32,4096]{1,0:T(8,128)} async-done(((f32[128,4096]{1,0:T(8,128)}), f32[32,4096]{1,0:T(8,128)}) %reduce-scatter.17.cloned.1.call-update) | async-done | bytes 524304 | tf_op jit(solution)/shard_map/reduce_scatter | solution.py:96
  217.0 1.9 multiply_convert_fusion
  218.8 0.0 all-gather.2.cloned.1.call-update
  218.9 0.0 copy-start.1
  218.9 0.0 all-reduce.6.cloned.1.call-start
  218.9 27.3 %all-gather.2.cloned.1.call-done = bf16[128,4096]{1,0:T(8,128)(2,1)} async-done(((bf16[32,4096]{1,0:T(8,128)(2,1)}), bf16[128,4096]{1,0:T(8,128)(2,1)}) %all-gather.2.cloned.1.call-update) | async-done | bytes 1048592 | tf_op jit(solution)/shard_map/all_gather | solution.py:104
  246.2 5.8 %fusion.31 = f32[128,1024]{1,0:T(8,128)} fusion(bf16[128,4096]{1,0:T(8,128)(2,1)} %all-gather.2.cloned.1.call-done, bf16[4096,1024]{1,0:T(8,128)(2,1)} %param.35), kind=kOutput, calls=%fused_computation.51 | convolution fusion | flops 1073741824 | bytes 9961472 | tf_op jit(solution)/shard_map/dot_general | solution.py:103
  252.0 0.0 all-reduce.6.cloned.1.call-update
  252.0 32.9 %all-reduce.6.cloned.1.call-done = f32[128,1024]{1,0:T(8,128)} async-done(((f32[128,1024]{1,0:T(8,128)}), f32[128,1024]{1,0:T(8,128)}) %all-reduce.6.cloned.1.call-update) | async-done | bytes 524304 | tf_op jit(solution)/shard_map/psum | solution.py:108
  284.9 1.8 fusion.7
  (20 shorter events, 0.0 us)
Async XLA Ops:
  6.5 7.5 %copy-start = (bf16[1024,1024]{1,0:T(8,128)(2,1)S(1)}, bf16[1024,1024]{1,0:T(8,128)(2,1)}, u32[]{:S(2)}) copy-start(bf16[1024,1024]{1,0:T(8,128)(2,1)} %param.27) | copy-start | bytes 6291460
  6.5 9.8 %copy-start.2 = (bf16[128,1024]{1,0:T(8,128)(2,1)S(1)}, bf16[128,1024]{1,0:T(8,128)(2,1)}, u32[]{:S(2)}) copy-start(bf16[128,1024]{1,0:T(8,128)(2,1)} %param.18) | copy-start | bytes 786436
  6.5 9.8 %copy-start.4 = (f32[1024]{0:T(1024)S(1)}, f32[1024]{0:T(1024)}, u32[]{:S(2)}) copy-start(f32[1024]{0:T(1024)} %param.24) | copy-start | bytes 12292
  6.5 26.4 %copy-start.8 = (s32[32]{0:T(128)S(1)}, s32[32]{0:T(128)}, u32[]{:S(2)}) copy-start(s32[32]{0:T(128)} %param.19) | copy-start | bytes 388
  6.5 34.7 %reduce-scatter.7.cloned.1.call-start = ((), (), s32[]{:S(2)}) async-start(), calls=%async_computation.6 | async-start | bytes 327680 | tf_op jit(solution)/shard_map/reduce_scatter | solution.py:46
  9.1 43.8 %reduce-scatter.11.cloned.1.call-start = ((), (), s32[]{:S(2)}) async-start(), calls=%async_computation.8 | async-start | bytes 327680 | tf_op jit(solution)/shard_map/reduce_scatter | solution.py:47
  11.5 61.9 %reduce-scatter.9.cloned.1.call-start = ((), (), s32[]{:S(2)}) async-start(), calls=%async_computation.7 | async-start | bytes 327680 | tf_op jit(solution)/shard_map/reduce_scatter | solution.py:50
  14.0 90.2 %reduce-scatter.13.cloned.1.call-start = ((), (), s32[]{:S(2)}) async-start(), calls=%async_computation.9 | async-start | bytes 655360 | tf_op jit(solution)/shard_map/reduce_scatter | solution.py:48
  16.2 101.7 %reduce-scatter.15.cloned.1.call-start = ((), (), s32[]{:S(2)}) async-start(), calls=%async_computation.10 | async-start | bytes 655360 | tf_op jit(solution)/shard_map/reduce_scatter | solution.py:49
  19.2 146.6 %all-reduce.4.cloned.1.call-start = ((), (), s32[]{:S(2)}) async-start(), calls=%async_computation.11 | async-start | bytes 1048576 | tf_op jit(solution)/shard_map/psum | solution.py:89
  33.2 40.2 %copy-start.6 = (f32[512]{0:T(512)S(1)}, f32[512]{0:T(512)}, u32[]{:S(2)}) copy-start(f32[512]{0:T(512)} %param.30) | copy-start | bytes 6148
  94.9 10.6 %copy-start.7 = (f32[64]{0:T(128)S(1)}, f32[64]{0:T(128)}, u32[]{:S(2)}) copy-start(f32[64]{0:T(128)} %param.31) | copy-start | bytes 772
  94.9 37.9 %copy-start.3 = (bf16[1024,1024]{1,0:T(8,128)(2,1)S(1)}, bf16[1024,1024]{1,0:T(8,128)(2,1)}, u32[]{:S(2)}) copy-start(bf16[1024,1024]{1,0:T(8,128)(2,1)} %param.32) | copy-start | bytes 6291460
  94.9 72.1 %copy-start.5 = (f32[1024]{0:T(1024)S(1)}, f32[1024]{0:T(1024)}, u32[]{:S(2)}) copy-start(f32[1024]{0:T(1024)} %param.33) | copy-start | bytes 12292
  134.1 82.9 %reduce-scatter.17.cloned.1.call-start = ((), (), s32[]{:S(2)}) async-start(), calls=%async_computation.12 | async-start | bytes 2621440 | tf_op jit(solution)/shard_map/reduce_scatter | solution.py:96
  167.0 6.1 %copy-start.9 = (u32[32]{0:T(128)S(1)}, u32[32]{0:T(128)}, u32[]{:S(2)}) copy-start(u32[32]{0:T(128)} %constant.44) | copy-start | bytes 388
  173.1 73.1 %all-gather.2.cloned.1.call-start = ((), (), s32[]{:S(2)}) async-start(), calls=%async_computation.13 | async-start | bytes 1310720 | tf_op jit(solution)/shard_map/all_gather | solution.py:104
  218.9 67.9 %copy-start.1 = (bf16[1024,1024]{1,0:T(8,128)(2,1)S(1)}, bf16[1024,1024]{1,0:T(8,128)(2,1)}, u32[]{:S(2)}) copy-start(bf16[1024,1024]{1,0:T(8,128)(2,1)} %param.27) | copy-start | bytes 6291460
  218.9 66.1 %all-reduce.6.cloned.1.call-start = ((), (), s32[]{:S(2)}) async-start(), calls=%async_computation.14 | async-start | bytes 1048576 | tf_op jit(solution)/shard_map/psum | solution.py:108
Sparse Core Ops, SparseCore 0:
  9.6 22.7 reduce-scatter.6
  34.6 18.2 reduce-scatter.10
  55.2 18.2 reduce-scatter.8
  75.6 20.1 reduce-scatter.12
  97.8 20.0 reduce-scatter.14
  134.2 31.5 all-reduce.3
  173.2 43.7 reduce-scatter.16
  219.0 27.1 all-gather.1
  252.1 32.7 all-reduce.5
where the time goes:
time: 294 us; the launch traced here: 293 us
  waiting for transfers between devices  167 us (57%)
  matrix products  44.8 us (15%)
  blocking collectives  39.5 us (13%)
  other arithmetic  26.6 us (9%)
  between operations  14 us (5%)
    psum x1, waiting for transfers between devices, shards(): mixer_out = lax.psum(down_terms, 'tp')  32.9 us
    psum x1, waiting for transfers between devices, shards(): attn_out = lax.psum(attn_terms, 'tp')  31.5 us
    reduce_scatter x1, waiting for transfers between devices, shards(): lax.psum_scatter(up_part, 'kv', scatter_dimension=0, tiled=True)  30.4 us
    all_gather x1, waiting for transfers between devices, shards(): lax.all_gather(hidden_share, 'kv', axis=0, tiled=True)  27.3 us
    reduce_scatter x1, waiting for transfers between devices, shards(): lax.psum_scatter(decay_part, 'kv', scatter_dimension=0, tiled=True)  20.5 us
    all_gather x1, blocking collectives, shards(): lax.all_gather(mixed, 'kv', axis=0, tiled=True)  13.8 us
    psum x1, blocking collectives, shards(): square_total = lax.psum(square_sum, 'kv')  13.6 us
    reduce_scatter x1, waiting for transfers between devices, shards(): lax.psum_scatter(gate_part, 'kv', scatter_dimension=0, tiled=True)  12.1 us
  transfers between devices with their start and end apart: 9, of which 7 were waited for; matrix products, arithmetic and copies ran while one was open for 17% of the time, Pallas kernels for 0%

commit v1 on v0

--- a/solution.py
+++ b/solution.py
@@ -8,6 +8,11 @@
 DV = 64
 NORM_EPS = 1e-06
 DECAY_SOFTNESS = 16.0
+
+
+def answer_counts(net_axis, matrix):
+    f_next = jnp.sum(lax.all_gather(matrix, axis_name=net_axis), axis=0)
+    return f_next
 
 
 def shards(
@@ -86,7 +91,7 @@
         out_weight,
         preferred_element_type=jnp.float32,
     )
-    attn_out = lax.psum(attn_terms, "tp")
+    attn_out = answer_counts("tp", attn_terms)
     resid = (whole_rows + attn_out).astype(jnp.bfloat16)
     resid_rows = resid.astype(jnp.float32)
     mixer_square = jnp.sum(resid_rows * resid_rows, axis=1)

time: 294 us -> 284 us (0.966)
  waiting for transfers between devices: 167 us -> 156 us
    psum x1 -> x0, waiting for transfers between devices: 31.5 us -> none  [shards(): attn_out = lax.psum(attn_terms, 'tp')]
    all_gather x0 -> x1, waiting for transfers between devices: none -> 20.7 us  [answer_counts(): f_next = jnp.sum(lax.all_gather(matrix, axis_name=net_axis), axis=0)]
  transfers between devices with their start and end apart: 9 -> 9, of which waited for: 7 -> 7; matrix products, arithmetic and copies ran while one was open for 17% -> 18% of each run, Pallas kernels for 0% -> 0%
where the time goes in v1:
time: 284 us; the launch traced here: 283 us
  waiting for transfers between devices  156 us (55%)
  matrix products  44.8 us (16%)
  blocking collectives  39.5 us (14%)
  other arithmetic  27.3 us (10%)
  between operations  14.1 us (5%)
    psum x1, waiting for transfers between devices, shards(): mixer_out = lax.psum(down_terms, 'tp')  32.9 us
    reduce_scatter x1, waiting for transfers between devices, shards(): lax.psum_scatter(up_part, 'kv', scatter_dimension=0, tiled=True)  30.4 us
    all_gather x1, waiting for transfers between devices, shards(): lax.all_gather(hidden_share, 'kv', axis=0, tiled=True)  27.3 us
    all_gather x1, waiting for transfers between devices, answer_counts(): f_next = jnp.sum(lax.all_gather(matrix, axis_name=net_axis), axis=0)  20.7 us
    reduce_scatter x1, waiting for transfers between devices, shards(): lax.psum_scatter(decay_part, 'kv', scatter_dimension=0, tiled=True)  20.5 us
    all_gather x1, blocking collectives, shards(): lax.all_gather(mixed, 'kv', axis=0, tiled=True)  13.8 us
    psum x1, blocking collectives, shards(): square_total = lax.psum(square_sum, 'kv')  13.6 us
    reduce_scatter x1, waiting for transfers between devices, shards(): lax.psum_scatter(gate_part, 'kv', scatter_dimension=0, tiled=True)  12.1 us
  transfers between devices with their start and end apart: 9, of which 7 were waited for; matrix products, arithmetic and copies ran while one was open for 18% of the time, Pallas kernels for 0%

profile of v1, /device:TPU:0, one launch (start us, length us, event | category | flops | bytes accessed | tf_op | source)
XLA Modules:
  0.0 283.2 jit_solution(9817129400817437764)
XLA Ops:
  6.5 0.0 reduce-scatter.7.cloned.1.call-start
  6.6 2.5 fusion.21
  9.1 0.0 reduce-scatter.7.cloned.1.call-update
  9.1 0.0 reduce-scatter.11.cloned.1.call-start
  9.2 2.4 fusion.17
  11.5 0.0 reduce-scatter.11.cloned.1.call-update
  11.5 0.0 reduce-scatter.9.cloned.1.call-start
  11.6 2.3 fusion.19
  13.9 0.0 reduce-scatter.9.cloned.1.call-update
  14.0 0.0 reduce-scatter.13.cloned.1.call-start
  14.0 2.2 fusion.15
  16.2 0.0 reduce-scatter.13.cloned.1.call-update
  16.2 0.0 reduce-scatter.15.cloned.1.call-start
  16.3 2.9 %fusion.13 = f32[128,1024]{1,0:T(8,128)} fusion(bf16[1024,1024]{1,0:T(8,128)(2,1)} %param.28, bf16[128,1024]{1,0:T(8,128)(2,1)S(1)} %copy-done.2, f32[1024]{0:T(1024)S(1)} %copy-done.4), kind=kOutput, calls=%fused_computation.29 | convolution fusion | flops 268828672 | bytes 2887680 | tf_op jit(solution)/shard_map/dot_general | solution.py:47
  19.2 0.0 reduce-scatter.15.cloned.1.call-update
  19.2 0.0 all-gather.6.cloned.1.call-start
  19.2 0.1 fusion.3
  19.4 13.6 %psum.14 = f32[128]{0:T(128)S(1)} all-reduce(f32[128]{0:T(128)S(1)} %fusion.3), channel_id=1, replica_groups=mesh['grp'=2,'kv'=4,'tp'=4] {'kv'}, use_global_device_ids=true, to_apply=%region_2.0 | all-reduce | flops 128 | bytes 1024 | tf_op jit(solution)/shard_map/psum | solution.py:49
  33.0 0.1 iota_compare_fusion
  33.0 0.1 iota_compare_fusion.1
  33.1 0.1 add_rsqrt_fusion.1
  33.2 8.0 %select_reduce_fusion = f32[32,512]{1,0:T(8,128)S(1)} fusion(f32[32,512,256]{2,1,0:T(8,128)} %param.23, pred[32,256]{1,0:T(8,128)(4,1)S(1)} %iota_compare_fusion.1), kind=kLoop, calls=%fused_computation.3 | loop fusion | flops 8372224 | bytes 16850944 | tf_op jit(solution)/shard_map/reduce_sum | solution.py:70
  41.2 0.0 reduce-scatter.7.cloned.1.call-done
  41.3 11.6 %reduce-scatter.11.cloned.1.call-done = f32[32,512]{1,0:T(8,128)} async-done(((f32[128,512]{1,0:T(8,128)}), f32[32,512]{1,0:T(8,128)}) %reduce-scatter.11.cloned.1.call-update) | async-done | bytes 65552 | tf_op jit(solution)/shard_map/reduce_scatter | solution.py:52
  52.9 20.5 %reduce-scatter.9.cloned.1.call-done = f32[32,512]{1,0:T(8,128)} async-done(((f32[128,512]{1,0:T(8,128)}), f32[32,512]{1,0:T(8,128)}) %reduce-scatter.9.cloned.1.call-update) | async-done | bytes 65552 | tf_op jit(solution)/shard_map/reduce_scatter | solution.py:55
  73.5 1.0 fusion.25
  74.5 0.1 reshape.83
  74.6 0.1 reshape.82
  74.7 0.1 reshape.86
  74.8 0.1 exponential_multiply_fusion
  75.0 9.7 %fusion.1 = bf16[32,16,256]{2,1,0:T(8,128)(2,1)S(1)} fusion(f32[32,16,32]{2,1,0:T(8,128)S(1)} %reshape.83, f32[32,16,32]{2,1,0:T(8,128)S(1)} %reshape.82, pred[32,256]{1,0:T(8,128)(4,1)S(1)} %iota_compare_fusion, bf16[32,512,256]{2,1,0:T(8,128)(2,1)} %param.21, f32[32,512,256]{2,1,0:T(8,128)} %param.23), kind=kLoop, calls=%fused_computation.2 | loop fusion | flops 25034752 | bytes 25567232 | tf_op jit(solution)/shard_map/reduce_sum | solution.py:76
  84.7 10.3 %fusion.8 = f32[32,16,1,64]{3,2,1,0:T(1,128)S(1)} fusion(bf16[32,16,64,256]{3,2,1,0:T(8,128)(2,1)} %bitcast.36, bf16[32,16,256,1]{2,1,0,3:T(8,128)(2,1)S(1)} %bitcast.34), kind=kOutput, calls=%fused_computation.16 | convolution fusion | flops 16777216 | bytes 17170432 | tf_op jit(solution)/shard_map/nhs,nhvs->nhv/dot_general | solution.py:79
  94.9 9.2 %fusion.29 = f32[32,16,1,64]{3,2,1,0:T(1,128)S(1)} fusion(f32[32,16,32,1]{2,3,1,0:T(1,128)S(1)} %bitcast.33, f32[32,16,32,64]{3,2,1,0:T(8,128)} %param.20), kind=kOutput, calls=%fused_computation.49 | convolution fusion | flops 12582912 | bytes 4390912 | tf_op jit(solution)/shard_map/nhc,nhcv->nhv/dot_general | solution.py:82
  104.2 0.0 reduce-scatter.13.cloned.1.call-done
  104.2 1.0 broadcast_multiply_fusion
  105.2 0.1 reshape.87
  105.3 0.2 multiply_reduce_fusion
  105.6 0.1 multiply_multiply_fusion
  105.7 0.1 reshape.88
  105.8 12.1 %reduce-scatter.15.cloned.1.call-done = f32[32,1024]{1,0:T(8,128)} async-done(((f32[128,1024]{1,0:T(8,128)}), f32[32,1024]{1,0:T(8,128)}) %reduce-scatter.15.cloned.1.call-update) | async-done | bytes 131088 | tf_op jit(solution)/shard_map/reduce_scatter | solution.py:54
  118.0 1.0 multiply_convert_fusion.1
  119.0 13.8 %all_gather.12 = bf16[128,1024]{1,0:T(8,128)(2,1)S(1)} all-gather(bf16[32,1024]{1,0:T(8,128)(2,1)S(1)} %multiply_convert_fusion.1), channel_id=1, replica_groups=mesh['grp'=2,'kv'=4,'tp'=4] {'kv'}, dimensions={0}, use_global_device_ids=true | all-gather | bytes 327680 | tf_op jit(solution)/shard_map/all_gather | solution.py:90
  132.8 1.2 fusion.30
  134.0 0.0 all-gather.6.cloned.1.call-update
  134.1 0.2 reduce-scatter.17.cloned.1.call-start
  134.3 20.7 %all-gather.6.cloned.1.call-done = f32[512,1024]{1,0:T(8,128)} async-done(((f32[128,1024]{1,0:T(8,128)}), f32[512,1024]{1,0:T(8,128)}) %all-gather.6.cloned.1.call-update) | async-done | bytes 2097168 | tf_op jit(solution)/shard_map/all_gather | solution.py:14
  155.0 1.8 reduce_sum.68
  156.8 0.2 fusion.6
  156.9 0.0 copy-start.9
  156.9 6.0 %fusion.10 = f32[128,4096]{1,0:T(8,128)} fusion(bf16[1024,4096]{1,0:T(8,128)(2,1)} %param.34, bf16[128,1024]{1,0:T(8,128)(2,1)S(1)} %get-tuple-element.6, f32[1024]{0:T(1024)S(1)} %copy-done.5), kind=kOutput, calls=%fused_computation.19 | convolution fusion | flops 1074135040 | bytes 10752000 | tf_op jit(solution)/shard_map/dot_general | solution.py:99
  162.9 0.0 reduce-scatter.17.cloned.1.call-update
  163.0 0.0 all-gather.4.cloned.1.call-start
  163.0 0.6 dynamic-slice
  164.3 12.1 %all-reduce = f32[128]{0:T(128)S(1)} all-reduce(f32[128]{0:T(128)S(1)} %get-tuple-element.5), channel_id=9, replica_groups=mesh['grp'=2,'kv'=4,'tp'=4] {'kv'}, use_global_device_ids=true, to_apply=%region_14.15.clone | all-reduce | flops 128 | bytes 1024
  176.4 0.1 fusion.27
  176.5 30.4 %reduce-scatter.17.cloned.1.call-done = f32[32,4096]{1,0:T(8,128)} async-done(((f32[128,4096]{1,0:T(8,128)}), f32[32,4096]{1,0:T(8,128)}) %reduce-scatter.17.cloned.1.call-update) | async-done | bytes 524304 | tf_op jit(solution)/shard_map/reduce_scatter | solution.py:101
  206.8 1.9 multiply_convert_fusion
  208.7 0.0 all-gather.4.cloned.1.call-update
  208.7 0.0 all-reduce.3.cloned.1.call-start
  208.8 27.3 %all-gather.4.cloned.1.call-done = bf16[128,4096]{1,0:T(8,128)(2,1)} async-done(((bf16[32,4096]{1,0:T(8,128)(2,1)}), bf16[128,4096]{1,0:T(8,128)(2,1)}) %all-gather.4.cloned.1.call-update) | async-done | bytes 1048592 | tf_op jit(solution)/shard_map/all_gather | solution.py:109
  236.1 5.8 %fusion.31 = f32[128,1024]{1,0:T(8,128)} fusion(bf16[128,4096]{1,0:T(8,128)(2,1)} %all-gather.4.cloned.1.call-done, bf16[4096,1024]{1,0:T(8,128)(2,1)} %param.35), kind=kOutput, calls=%fused_computation.51 | convolution fusion | flops 1073741824 | bytes 9961472 | tf_op jit(solution)/shard_map/dot_general | solution.py:108
  241.9 0.0 all-reduce.3.cloned.1.call-update
  241.9 32.9 %all-reduce.3.cloned.1.call-done = f32[128,1024]{1,0:T(8,128)} async-done(((f32[128,1024]{1,0:T(8,128)}), f32[128,1024]{1,0:T(8,128)}) %all-reduce.3.cloned.1.call-update) | async-done | bytes 524304 | tf_op jit(solution)/shard_map/psum | solution.py:113
  274.8 1.8 fusion.7
  (21 shorter events, 0.0 us)
Async XLA Ops:
  6.5 7.5 %copy-start = (bf16[1024,1024]{1,0:T(8,128)(2,1)S(1)}, bf16[1024,1024]{1,0:T(8,128)(2,1)}, u32[]{:S(2)}) copy-start(bf16[1024,1024]{1,0:T(8,128)(2,1)} %param.27) | copy-start | bytes 6291460
  6.5 9.8 %copy-start.2 = (bf16[128,1024]{1,0:T(8,128)(2,1)S(1)}, bf16[128,1024]{1,0:T(8,128)(2,1)}, u32[]{:S(2)}) copy-start(bf16[128,1024]{1,0:T(8,128)(2,1)} %param.18) | copy-start | bytes 786436
  6.5 9.8 %copy-start.4 = (f32[1024]{0:T(1024)S(1)}, f32[1024]{0:T(1024)}, u32[]{:S(2)}) copy-start(f32[1024]{0:T(1024)} %param.24) | copy-start | bytes 12292
  6.5 26.4 %copy-start.8 = (s32[32]{0:T(128)S(1)}, s32[32]{0:T(128)}, u32[]{:S(2)}) copy-start(s32[32]{0:T(128)} %param.19) | copy-start | bytes 388
  6.5 34.7 %reduce-scatter.7.cloned.1.call-start = ((), (), s32[]{:S(2)}) async-start(), calls=%async_computation.6 | async-start | bytes 327680 | tf_op jit(solution)/shard_map/reduce_scatter | solution.py:51
  9.1 43.8 %reduce-scatter.11.cloned.1.call-start = ((), (), s32[]{:S(2)}) async-start(), calls=%async_computation.8 | async-start | bytes 327680 | tf_op jit(solution)/shard_map/reduce_scatter | solution.py:52
  11.5 61.9 %reduce-scatter.9.cloned.1.call-start = ((), (), s32[]{:S(2)}) async-start(), calls=%async_computation.7 | async-start | bytes 327680 | tf_op jit(solution)/shard_map/reduce_scatter | solution.py:55
  14.0 90.2 %reduce-scatter.13.cloned.1.call-start = ((), (), s32[]{:S(2)}) async-start(), calls=%async_computation.9 | async-start | bytes 655360 | tf_op jit(solution)/shard_map/reduce_scatter | solution.py:53
  16.2 101.7 %reduce-scatter.15.cloned.1.call-start = ((), (), s32[]{:S(2)}) async-start(), calls=%async_computation.10 | async-start | bytes 655360 | tf_op jit(solution)/shard_map/reduce_scatter | solution.py:54
  19.2 135.8 %all-gather.6.cloned.1.call-start = ((), (), s32[]{:S(2)}) async-start(), calls=%async_computation.14 | async-start | bytes 2621440 | tf_op jit(solution)/shard_map/all_gather | solution.py:14
  33.2 40.2 %copy-start.6 = (f32[512]{0:T(512)S(1)}, f32[512]{0:T(512)}, u32[]{:S(2)}) copy-start(f32[512]{0:T(512)} %param.30) | copy-start | bytes 6148
  94.9 10.6 %copy-start.7 = (f32[64]{0:T(128)S(1)}, f32[64]{0:T(128)}, u32[]{:S(2)}) copy-start(f32[64]{0:T(128)} %param.31) | copy-start | bytes 772
  94.9 37.9 %copy-start.3 = (bf16[1024,1024]{1,0:T(8,128)(2,1)S(1)}, bf16[1024,1024]{1,0:T(8,128)(2,1)}, u32[]{:S(2)}) copy-start(bf16[1024,1024]{1,0:T(8,128)(2,1)} %param.32) | copy-start | bytes 6291460
  94.9 62.0 %copy-start.5 = (f32[1024]{0:T(1024)S(1)}, f32[1024]{0:T(1024)}, u32[]{:S(2)}) copy-start(f32[1024]{0:T(1024)} %param.33) | copy-start | bytes 12292
  134.1 72.8 %reduce-scatter.17.cloned.1.call-start = ((), (), s32[]{:S(2)}) async-start(), calls=%async_computation.11 | async-start | bytes 2621440 | tf_op jit(solution)/shard_map/reduce_scatter | solution.py:101
  156.9 6.1 %copy-start.9 = (u32[32]{0:T(128)S(1)}, u32[32]{0:T(128)}, u32[]{:S(2)}) copy-start(u32[32]{0:T(128)} %constant.44) | copy-start | bytes 388
  163.0 73.1 %all-gather.4.cloned.1.call-start = ((), (), s32[]{:S(2)}) async-start(), calls=%async_computation.12 | async-start | bytes 1310720 | tf_op jit(solution)/shard_map/all_gather | solution.py:109
  208.7 67.9 %copy-start.1 = (bf16[1024,1024]{1,0:T(8,128)(2,1)S(1)}, bf16[1024,1024]{1,0:T(8,128)(2,1)}, u32[]{:S(2)}) copy-start(bf16[1024,1024]{1,0:T(8,128)(2,1)} %param.27) | copy-start | bytes 6291460
  208.7 66.1 %all-reduce.3.cloned.1.call-start = ((), (), s32[]{:S(2)}) async-start(), calls=%async_computation.13 | async-start | bytes 1048576 | tf_op jit(solution)/shard_map/psum | solution.py:113
Sparse Core Ops, SparseCore 0:
  9.6 22.7 reduce-scatter.6
  34.6 18.2 reduce-scatter.10
  55.2 18.2 reduce-scatter.8
  75.6 20.1 reduce-scatter.12
  97.8 20.0 reduce-scatter.14
  134.2 20.7 all-gather.5
  163.1 43.7 reduce-scatter.16
  208.9 27.1 all-gather.3
  242.0 32.7 all-reduce.2
